TPU v7x, 32 devices: a whole 2x2x4 slice. The times are simulated.
32 devices in a mesh: sp: 16 (over z, y, core), tp: 2 (over x).
Axes of the slice: x: 2, y: 2, z: 4, core: 2. Of those that a mesh axis runs over, the one named last changes fastest.
Arguments:
- activations: bfloat16 [4096, 2048], P('sp', 'tp'), may hold values from -8 to 8
- norm_gain: float32 [2048], replicated, may hold values from 0.1 to 1.9
- win_query: bfloat16 [2048, 1024], P(None, 'tp'), may hold values from -1 to 1
- win_key: bfloat16 [2048, 512], P(None, 'tp'), may hold values from -1 to 1
- win_value: bfloat16 [2048, 512], P(None, 'tp'), may hold values from -0.125 to 0.125
- sink_logit: float32 [16], P('tp'), may hold values from 1 to 6
- lat_query: bfloat16 [2048, 1536], P(None, 'tp'), may hold values from -1 to 1
- key_value_down_weight: bfloat16 [2048, 128], replicated, may hold values from -0.125 to 0.125
- rope_key: bfloat16 [2048, 64], replicated, may hold values from -1 to 1
- latent_norm_gain: float32 [128], replicated, may hold values from 0.1 to 1.9
- key_up_weight: bfloat16 [128, 1024], P(None, 'tp'), may hold values from -0.5 to 0.5
- value_up_weight: bfloat16 [128, 1024], P(None, 'tp'), may hold values from -0.5 to 0.5
- out_win: bfloat16 [1024, 2048], P('tp'), may hold values from -0.359375 to 0.359375
- out_lat: bfloat16 [1024, 2048], P('tp'), may hold values from -0.59765625 to 0.59765625
Outputs:
- mixed: bfloat16 [4096, 2048], P('sp', 'tp')
All inputs are finite; a program needn't handle non-finite values.
Results may differ from a plain program's by a relative error of at most 0.025.
Values may be sent and summed in bfloat16 or wider, within the bound.
A program may use at most 64 MiB of HBM per device.

v0:
```python
from functools import partial

import jax
import jax.numpy as jnp
from jax import lax
from jax.sharding import PartitionSpec as P

HEADS_A = 16
DH = 64
WINDOW = 128
UNROTATED_WIDTH = 128
D_ROPE = 64
VALUE_WIDTH = 128


EPSILON = 1e-06
ROPE_BASE = 10000.0


def padded_2(cells, sides, width):
    for axis, dim in sides:
        count = lax.axis_size(axis)
        ends = count - 1
        head = lax.slice_in_dim(cells, 0, width, axis=dim)
        tail = lax.slice_in_dim(cells, cells.shape[dim] - width, cells.shape[dim], axis=dim)
        cells = jnp.concatenate(
            [
                lax.ppermute(tail, axis, [(i, (i + 1) % count) for i in range(ends)]),
                cells,
                lax.ppermute(head, axis, [((i + 1) % count, i) for i in range(ends)]),
            ],
            axis=dim,
        )
    return cells


def rotate(vectors, angles):
    half_width = vectors.shape[-1] // 2
    cosine_table = jnp.cos(angles)
    sine_table = jnp.sin(angles)
    lower_half = vectors[..., :half_width]
    upper_half = vectors[..., half_width:]
    return jnp.concatenate(
        [
            lower_half * cosine_table - upper_half * sine_table,
            lower_half * sine_table + upper_half * cosine_table,
        ],
        axis=-1,
    )


def rotary_angles(places, width):
    frequency = 1.0 / ROPE_BASE ** (jnp.arange(0, width, 2).astype(jnp.float32) / width)
    return places[:, None] * frequency[None, :]


def window_attention(queries, padded, sinks, offset, seq_total, head_start):
    tok_rows = queries.shape[0]
    key_heads = padded.shape[1] // (2 * DH)
    groups = queries.shape[1] // (DH * key_heads)
    key_rows = padded[:, : key_heads * DH].reshape(-1, key_heads, DH)
    value_rows = padded[:, key_heads * DH :].reshape(-1, key_heads, DH)
    grouped = queries.reshape(tok_rows, key_heads, groups, DH)
    scores = jnp.einsum(
        "qhgd,khd->hgqk", grouped, key_rows, preferred_element_type=jnp.float32
    ) * DH ** (-0.5)
    query_pos = offset + jnp.arange(tok_rows, dtype=jnp.int32)
    key_pos = offset - WINDOW + jnp.arange(tok_rows + 2 * WINDOW, dtype=jnp.int32)
    distance = jnp.abs(query_pos[:, None] - key_pos[None, :])
    in_window = (distance <= WINDOW) & (key_pos[None, :] >= 0) & (key_pos[None, :] < seq_total)
    head_ids = head_start + jnp.arange(key_heads * groups, dtype=jnp.int32)
    slopes = jnp.exp2(-8.0 * (head_ids + 1).astype(jnp.float32) / HEADS_A).reshape(
        key_heads, groups
    )
    scores = scores - slopes[:, :, None, None] * distance.astype(jnp.float32)[None, None]
    scores = jnp.where(in_window[None, None], scores, -jnp.inf)
    sink_table = sinks.reshape(key_heads, groups)
    row_peak = jnp.maximum(jnp.max(scores, axis=3), sink_table[:, :, None])
    weights = jnp.exp(scores - row_peak[..., None])
    denominator = jnp.sum(weights, axis=3) + jnp.exp(sink_table[:, :, None] - row_peak)
    blended = jnp.einsum(
        "hgqk,khd->qhgd",
        weights.astype(jnp.bfloat16),
        value_rows,
        preferred_element_type=jnp.float32,
    )
    blended = blended / jnp.transpose(denominator, (2, 0, 1))[..., None]
    return blended.reshape(tok_rows, key_heads * groups * DH).astype(jnp.bfloat16)


def latent_step(running, key_block, query_plain, query_turned):
    row_peak, totals, weighted = running
    keys_plain, values_plain, keys_turned = key_block
    key_count = keys_plain.shape[0]
    head_count = query_plain.shape[1]
    scores = jnp.einsum(
        "qhd,khd->hqk",
        query_plain,
        keys_plain.reshape(key_count, head_count, UNROTATED_WIDTH),
        preferred_element_type=jnp.float32,
    )
    scores = scores + jnp.einsum(
        "qhd,kd->hqk", query_turned, keys_turned, preferred_element_type=jnp.float32
    )
    scores = scores * (UNROTATED_WIDTH + D_ROPE) ** (-0.5)
    new_peak = jnp.maximum(row_peak, jnp.max(scores, axis=2))
    factor = jnp.exp(row_peak - new_peak)
    weights = jnp.exp(scores - new_peak[..., None])
    totals = totals * factor + jnp.sum(weights, axis=2)
    weighted = weighted * factor[..., None] + jnp.einsum(
        "hqk,khd->hqd",
        weights.astype(jnp.bfloat16),
        values_plain.reshape(key_count, head_count, VALUE_WIDTH),
        preferred_element_type=jnp.float32,
    )
    return (new_peak, totals, weighted)


def over_blocks(running, pieces, prepare, attend, block_rows):
    key_count = pieces[0].shape[0]
    stacked = tuple(
        (
            piece_part.reshape((key_count // block_rows, block_rows) + piece_part.shape[1:])
            for piece_part in pieces
        )
    )

    def one_block(state_now, key_block):
        return (attend(state_now, prepare(key_block)), None)

    return lax.scan(one_block, running, stacked)[0]


def per_device(
    activations,
    norm_gain,
    win_query,
    win_key,
    win_value,
    sink_logit,
    lat_query,
    key_value_down_weight,
    rope_key,
    latent_norm_gain,
    key_up_weight,
    value_up_weight,
    out_win,
    out_lat,
):
    tok_rows = activations.shape[0]
    weights_all = (win_query, win_key, win_value, lat_query, key_value_down_weight, rope_key)
    widened = lax.all_gather(activations, "tp", axis=1, tiled=True).astype(jnp.float32)
    normalized = (widened * norm_gain[None, :]).astype(jnp.bfloat16)
    squares = jnp.sum(widened * widened, axis=1)
    totals = tuple(
        (jnp.dot(normalized, weight, preferred_element_type=jnp.float32) for weight in weights_all)
    )
    squares, totals = (squares, totals)
    win_proj, key_proj, value_proj, latq_proj, compressed, rope_proj = totals
    row_scale = lax.rsqrt(squares / norm_gain.shape[0] + EPSILON)[:, None]
    offset = lax.axis_index("sp") * tok_rows
    seq_total = tok_rows * lax.axis_size("sp")
    places = (offset + jnp.arange(tok_rows, dtype=jnp.int32)).astype(jnp.float32)
    angles = rotary_angles(places, D_ROPE)
    win_queries = (win_proj * row_scale).astype(jnp.bfloat16)
    key_value = jnp.concatenate(
        [
            (key_proj * row_scale).astype(jnp.bfloat16),
            (value_proj * row_scale).astype(jnp.bfloat16),
        ],
        axis=1,
    )
    padded = padded_2(key_value, (("sp", 0),), WINDOW)
    head_start = lax.axis_index("tp") * sink_logit.shape[0]
    win_out = window_attention(win_queries, padded, sink_logit, offset, seq_total, head_start)
    head_count = lat_query.shape[1] // (UNROTATED_WIDTH + D_ROPE)
    query_all = (latq_proj * row_scale).reshape(tok_rows, head_count, UNROTATED_WIDTH + D_ROPE)
    query_plain = query_all[..., :UNROTATED_WIDTH].astype(jnp.bfloat16)
    query_turned = rotate(query_all[..., UNROTATED_WIDTH:], angles[:, None, :]).astype(jnp.bfloat16)
    latent = (
        compressed
        * lax.rsqrt(jnp.mean(compressed * compressed, axis=1, keepdims=True) + EPSILON)
        * latent_norm_gain[None, :]
    ).astype(jnp.bfloat16)
    key_rotary = rotate(rope_proj * row_scale, angles).astype(jnp.bfloat16)
    attend = partial(latent_step, query_plain=query_plain, query_turned=query_turned)

    def expand(key_block):
        return (
            jnp.dot(key_block[0], key_up_weight, preferred_element_type=jnp.float32).astype(
                jnp.bfloat16
            ),
            jnp.dot(key_block[0], value_up_weight, preferred_element_type=jnp.float32).astype(
                jnp.bfloat16
            ),
            key_block[1],
        )

    row_peak, totals_lat, weighted = over_blocks(
        (
            jnp.full((head_count, tok_rows), -jnp.inf, jnp.float32),
            jnp.zeros((head_count, tok_rows), jnp.float32),
            jnp.zeros((head_count, tok_rows, VALUE_WIDTH), jnp.float32),
        ),
        (
            lax.all_gather(latent, "sp", axis=0, tiled=True),
            lax.all_gather(key_rotary, "sp", axis=0, tiled=True),
        ),
        expand,
        attend,
        2048,
    )
    lat_out = (
        (weighted / totals_lat[..., None])
        .transpose(1, 0, 2)
        .reshape(tok_rows, head_count * VALUE_WIDTH)
    )
    lat_out = lat_out.astype(jnp.bfloat16)
    terms = jnp.dot(win_out, out_win, preferred_element_type=jnp.float32) + jnp.dot(
        lat_out, out_lat, preferred_element_type=jnp.float32
    )
    return lax.psum_scatter(terms.astype(jnp.bfloat16), "tp", scatter_dimension=1, tiled=True)


def solution(mesh):
    return jax.shard_map(
        per_device,
        mesh=mesh,
        in_specs=(
            P("sp", "tp"),
            P(),
            P(None, "tp"),
            P(None, "tp"),
            P(None, "tp"),
            P("tp"),
            P(None, "tp"),
            P(),
            P(),
            P(),
            P(None, "tp"),
            P(None, "tp"),
            P("tp", None),
            P("tp", None),
        ),
        out_specs=P("sp", "tp"),
        check_vma=False,
    )
```

profile of v0, /device:TPU:0, one launch (start us, length us, event | category | flops | bytes accessed | tf_op | source)
XLA Modules:
  0.0 175.6 jit_solution(10355702871223245682)
XLA Ops:
  7.3 0.9 max.19
  8.9 0.9 fusion.44
  9.8 0.9 fusion.41
  10.7 22.2 %all-gather.3.cloned.1.call-done = bf16[256,2048]{1,0:T(8,128)(2,1)} async-done(((bf16[256,1024]{1,0:T(8,128)(2,1)}), bf16[256,2048]{1,0:T(8,128)(2,1)}) %all-gather.3.cloned.1.call-update) | async-done | bytes 1048592 | tf_op jit(solution)/shard_map/all_gather | solution.py:152
  32.9 1.5 fusion.25
  34.5 3.1 %convolution_multiply_fusion = f32[256,768]{1,0:T(8,128)} fusion(bf16[2048,768]{1,0:T(8,128)(2,1)S(1)} %copy-done, bf16[256,2048]{1,0:T(8,128)(2,1)} %all-gather.3.cloned.1.call-done, f32[2048]{0:T(1024)} %param.17, f32[256]{0:T(256)S(1)} %add_rsqrt_fusion.1), kind=kOutput, calls=%fused_computation.38 | convolution fusion | flops 807075840 | bytes 4989952 | tf_op jit(solution)/shard_map/dot_general | solution.py:156
  37.6 2.3 %copy.30 = f32[256,768]{0,1:T(8,128)} copy(f32[256,768]{1,0:T(8,128)} %convolution_multiply_fusion) | data formatting | bytes 1572864 | tf_op jit(solution)/shard_map/mul | solution.py:177
  39.9 1.7 convolution_multiply_fusion.4
  41.8 22.9 %all_gather.11 = bf16[4096,64]{0,1:T(8,128)(2,1)S(1)} all-gather(bf16[256,64]{0,1:T(8,128)(2,1)S(1)} %pad_maximum_fusion.3), channel_id=1, replica_groups=mesh['sp'=16,'tp'=2] {'sp'}, dimensions={0}, use_global_device_ids=true | all-gather | bytes 557056 | tf_op jit(solution)/shard_map/all_gather | solution.py:207
  64.7 0.8 copy.44
  65.5 1.8 %slice.64 = bf16[256,4,128]{0,2,1:T(8,128)(2,1)} slice(f32[256,4,192]{0,2,1:T(8,128)} %bitcast.110), slice={[0:256], [0:4], [0:128]} | slice | bytes 524288 | tf_op jit(solution)/shard_map/slice | solution.py:178
  67.3 1.1 copy.32
  68.4 1.9 %multiply_reduce_fusion = (f32[256]{0:T(256)S(1)}, f32[256,128]{0,1:T(8,128)S(1)}) fusion(bf16[2048,128]{1,0:T(8,128)(2,1)} %param.23, bf16[256,2048]{1,0:T(8,128)(2,1)} %all-gather.3.cloned.1.call-done, f32[2048]{0:T(1024)} %param.17), kind=kOutput, calls=%fused_computation.67 | convolution fusion | flops 135855872 | bytes 1713152 | tf_op jit(solution)/shard_map/dot_general | solution.py:156
  70.3 1.4 multiply_convert_fusion
  71.8 2.3 %fusion.34 = bf16[256,256]{0,1:T(8,128)(2,1)S(1)} fusion(bf16[2048,256]{1,0:T(8,128)(2,1)} %param.20, bf16[256,2048]{1,0:T(8,128)(2,1)} %all-gather.3.cloned.1.call-done, f32[2048]{0:T(1024)} %param.17, f32[256]{0:T(256)S(1)} %copy-done.13), kind=kOutput, calls=%fused_computation.45 | convolution fusion | flops 270139392 | bytes 2237440 | tf_op jit(solution)/shard_map/dot_general | solution.py:156
  74.1 2.2 %fusion.33 = bf16[256,256]{0,1:T(8,128)(2,1)S(1)} fusion(bf16[2048,256]{1,0:T(8,128)(2,1)} %param.19, bf16[256,2048]{1,0:T(8,128)(2,1)} %all-gather.3.cloned.1.call-done, f32[2048]{0:T(1024)} %param.17, f32[256]{0:T(256)S(1)} %copy-done.13), kind=kOutput, calls=%fused_computation.44 | convolution fusion | flops 270139392 | bytes 2237440 | tf_op jit(solution)/shard_map/dot_general | solution.py:156
  77.0 2.9 %collective-permute-start = (bf16[128,512]{0,1:T(8,128)(2,1)}, bf16[128,512]{0,1:T(8,128)(2,1)}, u32[]{:S(2)}, u32[]{:S(2)}) collective-permute-start(bf16[128,512]{0,1:T(8,128)(2,1)} %get-tuple-element.141), channel_id=1, source_target_pairs={{0,2},{2,4},{4,6},{6,8},{8,10},{10,12},{12,14},{14,16},{16,18},{18... | collective-permute-start | bytes 393224 | tf_op jit(solution)/shard_map/ppermute | solution.py:28
  79.9 1.3 collective-permute-start.1
  81.2 1.4 fusion.32
  82.7 1.7 subtract_convert_fusion
  84.3 1.8 %copy.28 = bf16[256,512]{0,1:T(8,128)(2,1)} copy(bf16[256,512]{1,0:T(8,128)(2,1)} %fusion.32) | data formatting | bytes 524288 | tf_op jit(solution)/shard_map/convert_element_type | solution.py:165
  86.1 0.9 pad_maximum_fusion.2
  87.0 1.2 pad_maximum_fusion
  88.3 2.5 %fusion.23 = (f32[4,2,256]{2,1,0:T(2,128)S(1)}, f32[4,512,256,2]{2,1,3,0:T(8,128)S(1)}) fusion(f32[256,512]{0,1:T(8,128)} %fusion.41, f32[4,2]{1,0:T(4,128)S(1)} %copy-done.11, pred[256,512]{0,1:T(8,128)(4,1)} %fusion.44, bf16[512,4,64,1]{0,2,3,1:T(8,128)(2,1)S(1)} %bitcast.117, bf16[256,4,2,64]{0,3,2,1:T(8,128)(2,1)} %bitcast.115), kind=kOutput, calls=%fused_computation.33 | convolution fusion | flops 139458560 | bytes 5382176 | tf_op jit(solution)/shard_map/qhgd,khd->hgqk/dot_general | solution.py:64
  90.9 1.2 fusion.20
  92.2 1.4 fusion.38
  93.8 2.1 %fusion.61 = f32[256,2048]{1,0:T(8,128)} fusion(bf16[256,512]{0,1:T(8,128)(2,1)S(1)} %bitcast.114, bf16[512,2048]{1,0:T(8,128)(2,1)S(1)} %copy-done.6), kind=kOutput, calls=%fused_computation.89 | convolution fusion | flops 536870912 | bytes 4456448 | tf_op jit(solution)/shard_map/dot_general | solution.py:219
  95.9 9.1 %all-gather.5.cloned.1.call-done = bf16[4096,128]{0,1:T(8,128)(2,1)} async-done(((bf16[256,128]{0,1:T(8,128)(2,1)}), bf16[4096,128]{0,1:T(8,128)(2,1)}) %all-gather.5.cloned.1.call-update) | async-done | bytes 1048592 | tf_op jit(solution)/shard_map/all_gather | solution.py:206
  105.0 2.3 %copy.41 = bf16[4096,128]{1,0:T(8,128)(2,1)} copy(bf16[4096,128]{0,1:T(8,128)(2,1)} %all-gather.5.cloned.1.call-done) | data formatting | bytes 2097152
  107.3 34.6 %while.15 = (s32[]{:T(128)}, f32[4,256]{1,0:T(4,128)S(1)}, f32[4,256]{1,0:T(4,128)S(1)}, f32[4,256,128]{2,1,0:T(8,128)}, bf16[2,2048,128]{2,1,0:T(8,128)(2,1)}, ...) while((s32[]{:T(128)}, f32[4,256]{1,0:T(4,128)S(1)}, ...), condition=%wide.region_7.8_spmd.clone, body=%wide.region_4.7_spmd.clone.sunk | while | flops 1896223744 | bytes 93258992 | solution.py:131
  107.3 1.8 %convolution_convert_fusion.4 = bf16[2048,512]{0,1:T(8,128)(2,1)S(1)} fusion(bf16[128,512]{1,0:T(8,128)(2,1)} %get-tuple-element.255, bf16[2,2048,128]{2,1,0:T(8,128)(2,1)} %get-tuple-element.254, s32[]{:T(128)} %get-tuple-element.238), kind=kOutput, calls=%fused_computation.8.clone.1 | convolution fusion | flops 269484032 | bytes 2753024 | tf_op jit(solution)/shard_map/while/body/eval_jaxpr/dot_general | solution.py:190
  109.1 1.3 fusion.104
  110.4 4.5 %fusion.105 = (f32[4,256]{1,0:T(4,128)S(1)}, f32[4,256,2048]{1,2,0:T(8,128)}) fusion(bf16[256,4,64]{0,2,1:T(8,128)(2,1)S(1)} %get-tuple-element.258, bf16[2,2048,64]{1,2,0:T(8,128)(2,1)S(1)} %copy-done.4, s32[]{:T(128)} %get-tuple-element.238, f32[4,2048,256]{2,1,0:T(8,128)S(1)} %fusion.104), kind=kOutput, calls=%fused_computation.86.clone.1 | convolution fusion | flops 274725888 | bytes 17174532 | tf_op jit(solution)/shard_map/while/body/eval_jaxpr/qhd,kd->hqk/dot_general | solution.py:102
  114.9 4.6 %fusion.106 = f32[4,256]{1,0:T(4,128)S(1)} fusion(f32[4,256,2048]{1,2,0:T(8,128)} %get-tuple-element.223, f32[4,256]{1,0:T(4,128)S(1)} %select_maximum_fusion.2), kind=kLoop, calls=%fused_computation.4.clone.1 | loop fusion | flops 4193280 | bytes 8396800 | tf_op jit(solution)/shard_map/while/body/eval_jaxpr/reduce_sum | solution.py:109
  119.6 2.1 %convolution_convert_fusion.5 = bf16[2048,512]{0,1:T(8,128)(2,1)S(1)} fusion(bf16[128,512]{1,0:T(8,128)(2,1)} %get-tuple-element.259, bf16[2,2048,128]{2,1,0:T(8,128)(2,1)} %get-tuple-element.254, s32[]{:T(128)} %get-tuple-element.238), kind=kOutput, calls=%fused_computation.7.clone.1 | convolution fusion | flops 269484032 | bytes 2753024 | tf_op jit(solution)/shard_map/while/body/eval_jaxpr/dot_general | solution.py:193
  121.7 2.1 %fusion.108 = f32[4,256,128]{2,1,0:T(8,128)S(1)} fusion(bf16[2048,4,128]{0,2,1:T(8,128)(2,1)S(1)} %bitcast.106, f32[4,256,2048]{1,2,0:T(8,128)S(1)} %copy-done.1, f32[4,256]{1,0:T(4,128)S(1)} %select_maximum_fusion.2, f32[4,256,128]{2,1,0:T(8,128)S(1)} %copy-done.2, f32[4,256]{1,0:T(4,128)S(1)} %get-tuple-element.225, pred[]{:T(512)S(6)} %compare.3), kind=kOutput, calls=%fused_computation.9.clone.1 | convolution fusion | flops 541458432 | bytes 11542529 | tf_op jit(solution)/shard_map/while/body/eval_jaxpr/hqk,khd->hqd/dot_general | solution.py:110
  123.8 0.8 copy-done.3
  124.6 1.8 %convolution_convert_fusion.4 = bf16[2048,512]{0,1:T(8,128)(2,1)S(1)} fusion(bf16[128,512]{1,0:T(8,128)(2,1)} %get-tuple-element.255, bf16[2,2048,128]{2,1,0:T(8,128)(2,1)} %get-tuple-element.254, s32[]{:T(128)} %get-tuple-element.238), kind=kOutput, calls=%fused_computation.8.clone.1 | convolution fusion | flops 269484032 | bytes 2753024 | tf_op jit(solution)/shard_map/while/body/eval_jaxpr/dot_general | solution.py:190
  126.4 1.3 fusion.104
  127.7 4.5 %fusion.105 = (f32[4,256]{1,0:T(4,128)S(1)}, f32[4,256,2048]{1,2,0:T(8,128)}) fusion(bf16[256,4,64]{0,2,1:T(8,128)(2,1)S(1)} %get-tuple-element.258, bf16[2,2048,64]{1,2,0:T(8,128)(2,1)S(1)} %copy-done.4, s32[]{:T(128)} %get-tuple-element.238, f32[4,2048,256]{2,1,0:T(8,128)S(1)} %fusion.104), kind=kOutput, calls=%fused_computation.86.clone.1 | convolution fusion | flops 274725888 | bytes 17174532 | tf_op jit(solution)/shard_map/while/body/eval_jaxpr/qhd,kd->hqk/dot_general | solution.py:102
  132.2 4.6 %fusion.106 = f32[4,256]{1,0:T(4,128)S(1)} fusion(f32[4,256,2048]{1,2,0:T(8,128)} %get-tuple-element.223, f32[4,256]{1,0:T(4,128)S(1)} %select_maximum_fusion.2), kind=kLoop, calls=%fused_computation.4.clone.1 | loop fusion | flops 4193280 | bytes 8396800 | tf_op jit(solution)/shard_map/while/body/eval_jaxpr/reduce_sum | solution.py:109
  136.9 2.1 %convolution_convert_fusion.5 = bf16[2048,512]{0,1:T(8,128)(2,1)S(1)} fusion(bf16[128,512]{1,0:T(8,128)(2,1)} %get-tuple-element.259, bf16[2,2048,128]{2,1,0:T(8,128)(2,1)} %get-tuple-element.254, s32[]{:T(128)} %get-tuple-element.238), kind=kOutput, calls=%fused_computation.7.clone.1 | convolution fusion | flops 269484032 | bytes 2753024 | tf_op jit(solution)/shard_map/while/body/eval_jaxpr/dot_general | solution.py:193
  139.0 2.1 %fusion.108 = f32[4,256,128]{2,1,0:T(8,128)S(1)} fusion(bf16[2048,4,128]{0,2,1:T(8,128)(2,1)S(1)} %bitcast.106, f32[4,256,2048]{1,2,0:T(8,128)S(1)} %copy-done.1, f32[4,256]{1,0:T(4,128)S(1)} %select_maximum_fusion.2, f32[4,256,128]{2,1,0:T(8,128)S(1)} %copy-done.2, f32[4,256]{1,0:T(4,128)S(1)} %get-tuple-element.225, pred[]{:T(512)S(6)} %compare.3), kind=kOutput, calls=%fused_computation.9.clone.1 | convolution fusion | flops 541458432 | bytes 11542529 | tf_op jit(solution)/shard_map/while/body/eval_jaxpr/hqk,khd->hqd/dot_general | solution.py:110
  141.1 0.8 copy-done.3
  141.9 2.0 %copy.34 = f32[4,256,128]{1,2,0:T(8,128)} copy(f32[4,256,128]{2,1,0:T(8,128)} %get-tuple-element.58) | data formatting | bytes 1048576 | tf_op jit(solution)/shard_map/while | solution.py:131
  143.9 1.1 divide_convert_fusion
  145.0 3.9 %fusion.22 = bf16[256,2048]{1,0:T(8,128)(2,1)} fusion(f32[256,2048]{1,0:T(8,128)} %fusion.61, bf16[256,512]{0,1:T(8,128)(2,1)S(1)} %bitcast.113, bf16[512,2048]{1,0:T(8,128)(2,1)} %param.29), kind=kOutput, calls=%fused_computation.32 | convolution fusion | flops 537919488 | bytes 5505024 | tf_op jit(solution)/shard_map/dot_general | solution.py:219
  149.0 20.1 %reduce-scatter.2.cloned.1.call-done = bf16[256,1024]{1,0:T(8,128)(2,1)} async-done(((bf16[256,2048]{1,0:T(8,128)(2,1)}), bf16[256,1024]{1,0:T(8,128)(2,1)}) %reduce-scatter.2.cloned.1.call-update) | async-done | bytes 524304 | tf_op jit(solution)/shard_map/reduce_scatter | solution.py:222
  (70 shorter events, 2.9 us)
Async XLA Ops:
  6.5 27.9 %copy-start = (bf16[2048,768]{1,0:T(8,128)(2,1)S(1)}, bf16[2048,768]{1,0:T(8,128)(2,1)}, u32[]{:S(2)}) copy-start(bf16[2048,768]{1,0:T(8,128)(2,1)} %param.22) | copy-start | bytes 9437188
  6.5 26.4 %all-gather.3.cloned.1.call-start = ((), (), s32[]{:S(2)}) async-start(), calls=%async_computation.1 | async-start | bytes 1572864 | tf_op jit(solution)/shard_map/all_gather | solution.py:152
  7.3 97.8 %all-gather.5.cloned.1.call-start = ((), (), s32[]{:S(2)}) async-start(), calls=%async_computation.2 | async-start | bytes 1114112 | tf_op jit(solution)/shard_map/all_gather | solution.py:206
  10.7 29.1 %copy-start.15 = (f32[2048]{0:T(1024)S(1)}, f32[2048]{0:T(1024)}, u32[]{:S(2)}) copy-start(f32[2048]{0:T(1024)} %param.17) | copy-start | bytes 24580
  34.4 7.1 %copy-start.12 = (f32[256]{0:T(256)}, f32[256]{0:T(256)S(1)}, u32[]{:S(2)}) copy-start(f32[256]{0:T(256)S(1)} %add_rsqrt_fusion.1) | copy-start | bytes 3076
  41.8 30.0 %copy-start.13 = (f32[256]{0:T(256)S(1)}, f32[256]{0:T(256)}, u32[]{:S(2)}) copy-start(f32[256]{0:T(256)} %copy-done.12) | copy-start | bytes 3076
  65.5 15.7 %copy-start.16 = (f32[2048]{0:T(1024)S(1)}, f32[2048]{0:T(1024)}, u32[]{:S(2)}) copy-start(f32[2048]{0:T(1024)} %param.17) | copy-start | bytes 24580
  71.7 97.4 %reduce-scatter.2.cloned.1.call-start = ((), (), s32[]{:S(2)}) async-start(), calls=%async_computation.3 | async-start | bytes 1572864 | tf_op jit(solution)/shard_map/reduce_scatter | solution.py:222
  71.7 9.5 %copy-start.7 = (bf16[256,2048]{1,0:T(8,128)(2,1)S(1)}, bf16[256,2048]{1,0:T(8,128)(2,1)}, u32[]{:S(2)}) copy-start(bf16[256,2048]{1,0:T(8,128)(2,1)} %all-gather.3.cloned.1.call-done) | copy-start | bytes 3145732
  71.8 9.5 %copy-start.14 = (bf16[2048,512]{1,0:T(8,128)(2,1)S(1)}, bf16[2048,512]{1,0:T(8,128)(2,1)}, u32[]{:S(2)}) copy-start(bf16[2048,512]{1,0:T(8,128)(2,1)} %param.18) | copy-start | bytes 6291460
  74.0 8.6 %copy-start.9 = (bf16[256,256]{0,1:T(8,128)(2,1)}, bf16[256,256]{0,1:T(8,128)(2,1)S(1)}, u32[]{:S(2)}) copy-start(bf16[256,256]{0,1:T(8,128)(2,1)S(1)} %fusion.34) | copy-start | bytes 393220
  76.2 6.4 %copy-start.10 = (bf16[256,256]{0,1:T(8,128)(2,1)}, bf16[256,256]{0,1:T(8,128)(2,1)S(1)}, u32[]{:S(2)}) copy-start(bf16[256,256]{0,1:T(8,128)(2,1)S(1)} %fusion.33) | copy-start | bytes 393220
  76.3 12.0 %copy-start.11 = (f32[4,2]{1,0:T(4,128)S(1)}, f32[4,2]{1,0:T(4,128)}, u32[]{:S(2)}) copy-start(f32[4,2]{1,0:T(4,128)} %multiply_exponential_fusion) | copy-start | bytes 100
  77.0 10.0 %collective-permute-start = (bf16[128,512]{0,1:T(8,128)(2,1)}, bf16[128,512]{0,1:T(8,128)(2,1)}, u32[]{:S(2)}, u32[]{:S(2)}) collective-permute-start(bf16[128,512]{0,1:T(8,128)(2,1)} %get-tuple-element.141), channel_id=1, source_target_pairs={{0,2},{2,4},{4,6},{6,8},{8,10},{10,12},{12,14},{14,16},{16,18},{18... | collective-permute-start | bytes 393224 | tf_op jit(solution)/shard_map/ppermute | solution.py:28
  79.9 7.1 %collective-permute-start.1 = (bf16[128,512]{0,1:T(8,128)(2,1)}, bf16[128,512]{0,1:T(8,128)(2,1)}, u32[]{:S(2)}, u32[]{:S(2)}) collective-permute-start(bf16[128,512]{0,1:T(8,128)(2,1)} %get-tuple-element.142), channel_id=1, source_target_pairs={{2,0},{4,2},{6,4},{8,6},{10,8},{12,10},{14,12},{16,14},{18,16},{20... | collective-permute-start | bytes 393224 | tf_op jit(solution)/shard_map/ppermute | solution.py:30
  87.0 3.9 %copy-start.5 = (f32[256,512]{0,1:T(8,128)S(1)}, f32[256,512]{0,1:T(8,128)}, u32[]{:S(2)}) copy-start(f32[256,512]{0,1:T(8,128)} %fusion.41) | copy-start | bytes 1572868
  87.0 3.9 %copy-start.8 = (pred[256,512]{0,1:T(8,128)(4,1)S(1)}, pred[256,512]{0,1:T(8,128)(4,1)}, u32[]{:S(2)}) copy-start(pred[256,512]{0,1:T(8,128)(4,1)} %fusion.44) | copy-start | bytes 393220
  92.2 1.6 copy-start.6
  109.1 1.3 copy-start.4
  114.9 6.7 %copy-start.1 = (f32[4,256,2048]{1,2,0:T(8,128)S(1)}, f32[4,256,2048]{1,2,0:T(8,128)}, u32[]{:S(2)}) copy-start(f32[4,256,2048]{1,2,0:T(8,128)} %get-tuple-element.223) | copy-start | bytes 25165828 | tf_op jit(solution)/shard_map/while
  114.9 6.7 %copy-start.2 = (f32[4,256,128]{2,1,0:T(8,128)S(1)}, f32[4,256,128]{2,1,0:T(8,128)}, u32[]{:S(2)}) copy-start(f32[4,256,128]{2,1,0:T(8,128)} %get-tuple-element.241) | copy-start | bytes 1572868 | tf_op jit(solution)/shard_map/while
  123.8 0.8 copy-start.3
  126.4 1.3 copy-start.4
  132.2 6.7 %copy-start.1 = (f32[4,256,2048]{1,2,0:T(8,128)S(1)}, f32[4,256,2048]{1,2,0:T(8,128)}, u32[]{:S(2)}) copy-start(f32[4,256,2048]{1,2,0:T(8,128)} %get-tuple-element.223) | copy-start | bytes 25165828 | tf_op jit(solution)/shard_map/while
  132.2 6.7 %copy-start.2 = (f32[4,256,128]{2,1,0:T(8,128)S(1)}, f32[4,256,128]{2,1,0:T(8,128)}, u32[]{:S(2)}) copy-start(f32[4,256,128]{2,1,0:T(8,128)} %get-tuple-element.241) | copy-start | bytes 1572868 | tf_op jit(solution)/shard_map/while
  141.1 0.8 copy-start.3
Sparse Core Ops, SparseCore 0:
  8.9 23.9 all-gather.2
  71.8 33.1 all-gather.4
  149.1 19.9 reduce-scatter.1
where the time goes:
time: 176 us
  waiting for transfers between devices  52.2 us (30%)
  matrix products  46 us (26%)
  blocking collectives  22.9 us (13%)
  other arithmetic  21.9 us (12%)
  local copies, waits for them, and re-layouts  14.9 us (8%)
  between operations  13.4 us (8%)
  starting transfers between devices  4.27 us (2%)
    all_gather x1, blocking collectives, per_device(): lax.all_gather(key_rotary, 'sp', axis=0, tiled=True)  22.9 us
    all_gather x1, waiting for transfers between devices, per_device(): lax.all_gather(activations, 'tp', axis=1, tiled=True).astype(jnp.float32)  22.2 us
    reduce_scatter x1, waiting for transfers between devices, per_device(): lax.psum_scatter(terms.astype(jnp.bfloat16), 'tp', scatter_dimension=1, t...  20.1 us
    dot_general x6, matrix products, per_device(): jnp.dot(normalized, weight, preferred_element_type=jnp.float32)  12.6 us
    reduce_sum x2, other arithmetic, latent_step(): totals = totals * factor + jnp.sum(weights, axis=2)  9.28 us
    all_gather x1, waiting for transfers between devices, per_device(): lax.all_gather(latent, 'sp', axis=0, tiled=True)  9.12 us
    dot_general x2, matrix products, latent_step(): jnp.einsum('qhd,kd->hqk', query_turned, keys_turned, preferred_element_ty...  9.05 us
    dot_general x2, matrix products, latent_step(): jnp.einsum('hqk,khd->hqd', weights.astype(jnp.bfloat16), values_plain.res...  4.13 us
  transfers between devices with their start and end apart: 5, of which 3 were waited for; matrix products, arithmetic and copies ran while one was open for 13% of the time, Pallas kernels for 0%

commit v1 on v0

v1 whole, which is shorter than its diff:
```python
import functools

import jax
import jax.numpy as jnp
import numpy as np
from jax import lax
from jax.experimental import pallas as pl
from jax.experimental.pallas import tpu as pltpu
from jax.sharding import PartitionSpec as P

HEADS_A = 16
DH = 64
WINDOW = 128
UNROTATED_WIDTH = 128
D_ROPE = 64
VALUE_WIDTH = 128

EPSILON = 1e-06
ROPE_BASE = 10000.0
LOG2E = 1.4426950408889634
MESH = pl.DeviceIdType.MESH
F32 = jnp.float32
BF16 = jnp.bfloat16
SUB = 2


def turn(vectors, cosine, sine):
    half = vectors.shape[-1] // 2
    swapped = jnp.concatenate([vectors[:, half:], vectors[:, :half]], axis=1)
    return vectors * cosine + swapped * sine


def dot_nt(a, b):
    return lax.dot_general(a, b, (((1,), (1,)), ((), ())), preferred_element_type=F32)


def project_kernel(
    n_sp, n_tp,
    x_ref, gain_ref, cos_ref, sin_ref, sink_ref, slope_ref, lng_ref, kup_ref,
    wkv_hbm, wr_hbm, wk_hbm, wv_hbm, wq_hbm, wlq_hbm,
    q_ref, kv_ref, win_ref,
    x_all, wkv, wr, wk, wv, wq, wlq, akv, ar, ak, av, aq, alq, sq, gath, halo, qwin,
    w_sem, x_send, x_recv, z_send, z_recv, y_send, y_recv, c_send, c_recv, h_send, h_recv,
):
    sp = lax.axis_index("sp")
    tp = lax.axis_index("tp")
    rows, local = x_ref.shape
    part = local // SUB
    hi = n_sp // 4
    z, y, c = sp // 4, (sp // 2) % 2, sp % 2

    def at(zz, yy, cc):
        return (zz * 2 + yy) * 2 + cc

    right, left = (sp + 1) % n_sp, (sp + n_sp - 1) % n_sp

    weights = ((wkv_hbm, wkv), (wr_hbm, wr), (wk_hbm, wk), (wv_hbm, wv), (wq_hbm, wq), (wlq_hbm, wlq))
    loads = [pltpu.make_async_copy(a, b, w_sem.at[i]) for i, (a, b) in enumerate(weights)]
    for load in loads:
        load.start()

    barrier = pltpu.get_barrier_semaphore()
    peers = [(sp, (tp + s) % n_tp) for s in range(1, n_tp)]
    peers += [(at((z + d) % hi, y, c), tp) for d in range(1, hi)]
    peers += [(at(z, 1 - y, c), tp), (at(z, y, 1 - c), tp), (right, tp), (left, tp)]
    for peer in peers:
        pl.semaphore_signal(barrier, inc=1, device_id=peer, device_id_type=MESH)
    pl.semaphore_wait(barrier, len(peers))

    def remote(src, dst, send, recv, device):
        return pltpu.make_async_remote_copy(
            src_ref=src, dst_ref=dst, send_sem=send, recv_sem=recv, device_id=device, device_id_type=MESH
        )

    x_copies = {}
    for cc in range(SUB):
        for s in range(1, n_tp):
            x_copies[s, cc] = remote(
                x_ref.at[:, cc * part : (cc + 1) * part],
                x_all.at[tp * SUB + cc],
                x_send.at[s, cc],
                x_recv.at[s, cc],
                (sp, (tp + s) % n_tp),
            )
            x_copies[s, cc].start()

    def add_in(block, slot, pairs, first):
        where = pl.ds(pl.multiple_of(slot * part, part), part)
        for weight, acc in pairs:
            term = jnp.dot(block, weight[where, :], preferred_element_type=F32)
            acc[...] = term if first else acc[...] + term

    def norm_block(raw, slot, first):
        wide = raw.astype(F32)
        total = jnp.broadcast_to(jnp.sum(wide * wide, axis=1, keepdims=True), sq.shape)
        sq[...] = total if first else sq[...] + total
        return (wide * gain_ref[slot]).astype(BF16)

    small = ((wkv, akv), (wr, ar))
    big = ((wk, ak), (wv, av), (wq, aq), (wlq, alq))
    for load in loads:
        load.wait()
    for cc in range(SUB):
        slot = tp * SUB + cc
        block = norm_block(x_ref[:, cc * part : (cc + 1) * part], slot, cc == 0)
        add_in(block, slot, small + big, cc == 0)
    steps = [(s, cc) for cc in range(SUB) for s in range(1, n_tp)]
    for s, cc in steps[:-1]:
        x_copies[s, cc].wait_recv()
        slot = ((tp + n_tp - s) % n_tp) * SUB + cc
        add_in(norm_block(x_all[slot], slot, False), slot, small + big, False)
    s, cc = steps[-1]
    x_copies[s, cc].wait_recv()
    last_slot = ((tp + n_tp - s) % n_tp) * SUB + cc
    last_block = norm_block(x_all[last_slot], last_slot, False)
    add_in(last_block, last_slot, small, False)

    scale = lax.rsqrt(sq[:, 0:1] / (local * n_tp) + EPSILON)
    comp = akv[...]
    latent = comp * lax.rsqrt(jnp.mean(comp * comp, axis=1, keepdims=True) + EPSILON) * lng_ref[...]
    rotary = turn(ar[...] * scale, cos_ref[...], sin_ref[...])
    gath[sp, 0:rows, :] = latent.astype(BF16)
    gath[sp, rows : rows + rows // 2, :] = jnp.concatenate(
        [rotary[: rows // 2], rotary[rows // 2 :]], axis=1
    ).astype(BF16)

    def forward(block, sends, recvs, index, device):
        copy = remote(gath.at[block], gath.at[block], sends.at[index], recvs.at[index], device)
        copy.start()
        return copy

    to_y, to_c = (at(z, 1 - y, c), tp), (at(z, y, 1 - c), tp)
    z_copies = [forward(sp, z_send, z_recv, d, (at((z + d) % hi, y, c), tp)) for d in range(1, hi)]
    y_copies = [forward(sp, y_send, y_recv, 0, to_y)]
    c_copies = [forward(sp, c_send, c_recv, 0, to_c)]

    add_in(last_block, last_slot, big, False)
    k_cols = ak.shape[1]
    halo[WINDOW : WINDOW + rows, 0:k_cols] = (ak[...] * scale).astype(BF16)
    halo[WINDOW : WINDOW + rows, k_cols : 2 * k_cols] = (av[...] * scale).astype(BF16)
    h_copies = [
        remote(halo.at[rows : rows + WINDOW], halo.at[0:WINDOW], h_send.at[0], h_recv.at[0], (right, tp)),
        remote(
            halo.at[WINDOW : 2 * WINDOW],
            halo.at[rows + WINDOW : rows + 2 * WINDOW],
            h_send.at[1],
            h_recv.at[1],
            (left, tp),
        ),
    ]
    for copy in h_copies:
        copy.start()
    qwin[...] = (aq[...] * scale).astype(BF16)
    per_head = UNROTATED_WIDTH + D_ROPE
    factor = per_head ** (-0.5) * LOG2E
    for h in range(alq.shape[1] // per_head):
        one = alq[:, h * per_head : (h + 1) * per_head] * scale
        plain = one[:, :UNROTATED_WIDTH].astype(BF16)
        seen = dot_nt(plain, kup_ref[:, h * UNROTATED_WIDTH : (h + 1) * UNROTATED_WIDTH]) * factor
        turned = turn(one[:, UNROTATED_WIDTH:], cos_ref[...], sin_ref[...]) * factor
        q_ref[h, :, 0:UNROTATED_WIDTH] = seen.astype(BF16)
        q_ref[h, :, UNROTATED_WIDTH:] = jnp.concatenate([turned, jnp.zeros_like(turned)], axis=1).astype(BF16)

    for d in range(1, hi):
        z_copies[d - 1].wait_recv()
        block = at((z + hi - d) % hi, y, c)
        y_copies.append(forward(block, y_send, y_recv, d, to_y))
        c_copies.append(forward(block, c_send, c_recv, d, to_c))
    for copy in h_copies:
        copy.wait()

    span = 3 * WINDOW
    spots = lax.broadcasted_iota(jnp.int32, (WINDOW, span), 0)
    keys_at = lax.broadcasted_iota(jnp.int32, (WINDOW, span), 1)
    distance = jnp.abs(spots + WINDOW - keys_at)
    far = distance.astype(F32)
    seq_total = rows * n_sp

    def window(kv_head):
        for b in range(rows // WINDOW):
            key_pos = sp * rows + (b - 1) * WINDOW + keys_at
            inside = (distance <= WINDOW) & (key_pos >= 0) & (key_pos < seq_total)
            keys = halo[b * WINDOW : b * WINDOW + span, kv_head * DH : (kv_head + 1) * DH]
            values = halo[b * WINDOW : b * WINDOW + span, k_cols + kv_head * DH : k_cols + (kv_head + 1) * DH]
            pieces = []
            for g in range(2):
                head = kv_head * 2 + g
                query = qwin[b * WINDOW : (b + 1) * WINDOW, head * DH : (head + 1) * DH]
                scores = dot_nt(query, keys) * DH ** (-0.5) - slope_ref[head] * far
                scores = jnp.where(inside, scores, -jnp.inf)
                peak = jnp.maximum(jnp.max(scores, axis=1, keepdims=True), sink_ref[head])
                weight = jnp.exp(scores - peak)
                bottom = jnp.sum(weight, axis=1, keepdims=True) + jnp.exp(sink_ref[head] - peak)
                blended = jnp.dot(weight.astype(BF16), values, preferred_element_type=F32)
                pieces.append(blended / bottom)
            win_ref[b * WINDOW : (b + 1) * WINDOW, kv_head * 2 * DH : (kv_head + 1) * 2 * DH] = (
                jnp.concatenate(pieces, axis=1).astype(BF16)
            )

    kv_heads = k_cols // DH
    for kv_head in range((kv_heads + 1) // 2):
        window(kv_head)
    for d in range(hi):
        y_copies[d].wait_recv()
        c_copies.append(forward(at((z + hi - d) % hi, 1 - y, c), c_send, c_recv, hi + d, to_c))
    for kv_head in range((kv_heads + 1) // 2, kv_heads):
        window(kv_head)

    lanes = lax.broadcasted_iota(jnp.int32, (rows // 2, D_ROPE), 1)
    mark = jnp.where(lanes == 0, 1.0, 0.0).astype(BF16)

    def assemble(block):
        base = pl.multiple_of(block * rows, rows)
        kv_ref[pl.ds(base, rows), 0:UNROTATED_WIDTH] = gath[block, 0:rows, :]
        both = gath[block, rows : rows + rows // 2, :]
        kv_ref[pl.ds(base, rows // 2), UNROTATED_WIDTH:] = jnp.concatenate([both[:, :D_ROPE], mark], axis=1)
        kv_ref[pl.ds(base + rows // 2, rows // 2), UNROTATED_WIDTH:] = jnp.concatenate(
            [both[:, D_ROPE:], mark], axis=1
        )

    for d in range(hi):
        assemble(at((z + hi - d) % hi, y, c))
        assemble(at((z + hi - d) % hi, 1 - y, c))
    for d in range(hi):
        c_copies[d].wait_recv()
        assemble(at((z + hi - d) % hi, y, 1 - c))
    for d in range(hi):
        c_copies[hi + d].wait_recv()
        assemble(at((z + hi - d) % hi, 1 - y, 1 - c))
    for copy in list(x_copies.values()) + z_copies + y_copies + c_copies:
        copy.wait_send()


def attend_kernel(
    n_tp,
    q_ref, kv_ref, win_ref, vup_ref, ow_hbm, ol_hbm,
    out_ref,
    ow, ol, acc, peak, lat, outgoing, incoming, own, w_sem, send, recv,
):
    sp = lax.axis_index("sp")
    tp = lax.axis_index("tp")
    heads, rows, _ = q_ref.shape
    half = rows // 2
    cols = out_ref.shape[1]
    loads = [pltpu.make_async_copy(ow_hbm, ow, w_sem.at[0]), pltpu.make_async_copy(ol_hbm, ol, w_sem.at[1])]
    for load in loads:
        load.start()
    barrier = pltpu.get_barrier_semaphore()
    for s in range(1, n_tp):
        pl.semaphore_signal(barrier, inc=1, device_id=(sp, (tp + s) % n_tp), device_id_type=MESH)
    pl.semaphore_wait(barrier, n_tp - 1)

    chunk = min(1024, kv_ref.shape[0])
    copies = []
    for b in range(2):
        query = jnp.concatenate([q_ref[h, b * half : (b + 1) * half, :] for h in range(heads)], axis=0)
        acc[...] = jnp.zeros_like(acc)
        peak[...] = jnp.full_like(peak, -jnp.inf)

        def step(i, carry):
            keys = kv_ref[pl.ds(pl.multiple_of(i * chunk, chunk), chunk), :]
            scores = dot_nt(query, keys)
            old = peak[:, 0:1]
            new = jnp.maximum(old, jnp.max(scores, axis=1, keepdims=True))
            weight = jnp.exp2(scores - new).astype(BF16)
            acc[...] = acc[...] * jnp.exp2(old - new) + jnp.dot(weight, keys, preferred_element_type=F32)
            peak[...] = jnp.broadcast_to(new, peak.shape)
            return carry

        lax.fori_loop(0, kv_ref.shape[0] // chunk, step, 0)
        bottom = acc[:, UNROTATED_WIDTH + D_ROPE : UNROTATED_WIDTH + D_ROPE + 1]
        blended = (acc[:, 0:VALUE_WIDTH] / bottom).astype(BF16)
        for h in range(heads):
            where = slice(h * VALUE_WIDTH, (h + 1) * VALUE_WIDTH)
            lat[:, where] = jnp.dot(
                blended[h * half : (h + 1) * half], vup_ref[:, where], preferred_element_type=F32
            ).astype(BF16)
        if b == 0:
            for load in loads:
                load.wait()
        won = win_ref[b * half : (b + 1) * half, :]

        def terms(j):
            where = pl.ds(pl.multiple_of(j * cols, cols), cols)
            return jnp.dot(won, ow[:, where], preferred_element_type=F32) + jnp.dot(
                lat[...], ol[:, where], preferred_element_type=F32
            )

        for s in range(1, n_tp):
            other = (tp + s) % n_tp
            outgoing[b, s - 1] = terms(other).astype(BF16)
            copy = pltpu.make_async_remote_copy(
                src_ref=outgoing.at[b, s - 1],
                dst_ref=incoming.at[b, s - 1],
                send_sem=send.at[b, s],
                recv_sem=recv.at[b, s],
                device_id=(sp, other),
                device_id_type=MESH,
            )
            copy.start()
            copies.append((b, s, copy))
        own[b] = terms(tp)
    for b in range(2):
        total = own[b]
        for bb, s, copy in copies:
            if bb == b:
                copy.wait()
                total = total + incoming[b, s - 1].astype(F32)
        out_ref[b * half : (b + 1) * half, :] = total.astype(BF16)


def per_device(
    n_sp, n_tp,
    activations, norm_gain, win_query, win_key, win_value, sink_logit, lat_query,
    key_value_down_weight, rope_key, latent_norm_gain, key_up_weight, value_up_weight, out_win, out_lat,
):
    rows, local = activations.shape
    width = local * n_tp
    part = local // SUB
    heads_a = sink_logit.shape[0]
    heads_l = lat_query.shape[1] // (UNROTATED_WIDTH + D_ROPE)
    places = (lax.axis_index("sp") * rows + jnp.arange(rows, dtype=jnp.int32)).astype(F32)
    frequency = 1.0 / ROPE_BASE ** (jnp.arange(0, D_ROPE, 2).astype(F32) / D_ROPE)
    angles = places[:, None] * frequency[None, :]
    cosine, sine = jnp.cos(angles), jnp.sin(angles)
    cosine = jnp.concatenate([cosine, cosine], axis=1)
    sine = jnp.concatenate([-sine, sine], axis=1)
    head_ids = lax.axis_index("tp") * heads_a + jnp.arange(heads_a, dtype=jnp.int32)
    slopes = jnp.exp2(-8.0 * (head_ids + 1).astype(F32) / HEADS_A)

    vmem = pl.BlockSpec(memory_space=pltpu.VMEM)
    smem = pl.BlockSpec(memory_space=pltpu.SMEM)
    hbm = pl.BlockSpec(memory_space=pl.ANY)
    weights = (key_value_down_weight, rope_key, win_key, win_value, win_query, lat_query)
    hi = n_sp // 4
    dma = pltpu.SemaphoreType.DMA
    packed = rows + rows // 2
    query, keys, win_out = pl.pallas_call(
        functools.partial(project_kernel, n_sp, n_tp),
        out_shape=(
            jax.ShapeDtypeStruct((heads_l, rows, 2 * UNROTATED_WIDTH), BF16),
            jax.ShapeDtypeStruct((rows * n_sp, 2 * UNROTATED_WIDTH), BF16),
            jax.ShapeDtypeStruct((rows, heads_a * DH), BF16),
        ),
        in_specs=[vmem, vmem, vmem, vmem, smem, smem, vmem, vmem] + [hbm] * 6,
        out_specs=(vmem, vmem, vmem),
        scratch_shapes=[pltpu.VMEM((n_tp * SUB, rows, part), BF16)]
        + [pltpu.VMEM(w.shape, BF16) for w in weights]
        + [pltpu.VMEM((rows, w.shape[1]), F32) for w in weights]
        + [
            pltpu.VMEM((rows, 128), F32),
            pltpu.VMEM((n_sp, packed, UNROTATED_WIDTH), BF16),
            pltpu.VMEM((rows + 2 * WINDOW, 2 * win_key.shape[1]), BF16),
            pltpu.VMEM((rows, win_query.shape[1]), BF16),
            dma((6,)),
            dma((n_tp, SUB)), dma((n_tp, SUB)),
            dma((hi,)), dma((hi,)),
            dma((hi,)), dma((hi,)),
            dma((2 * hi,)), dma((2 * hi,)),
            dma((2,)), dma((2,)),
        ],
        compiler_params=pltpu.CompilerParams(
            collective_id=0, has_side_effects=True, vmem_limit_bytes=56 * 1024 * 1024
        ),
        name="project",
    )(
        activations, norm_gain.reshape(n_tp * SUB, 1, part), cosine, sine, sink_logit, slopes,
        latent_norm_gain.reshape(1, -1), key_up_weight, *weights,
    )
    return pl.pallas_call(
        functools.partial(attend_kernel, n_tp),
        out_shape=jax.ShapeDtypeStruct((rows, width // n_tp), BF16),
        in_specs=[vmem, vmem, vmem, vmem, hbm, hbm],
        out_specs=vmem,
        scratch_shapes=[
            pltpu.VMEM(out_win.shape, BF16),
            pltpu.VMEM(out_lat.shape, BF16),
            pltpu.VMEM((heads_l * rows // 2, 2 * UNROTATED_WIDTH), F32),
            pltpu.VMEM((heads_l * rows // 2, 128), F32),
            pltpu.VMEM((rows // 2, heads_l * VALUE_WIDTH), BF16),
            pltpu.VMEM((2, n_tp - 1, rows // 2, width // n_tp), BF16),
            pltpu.VMEM((2, n_tp - 1, rows // 2, width // n_tp), BF16),
            pltpu.VMEM((2, rows // 2, width // n_tp), F32),
            dma((2,)),
            dma((2, n_tp)), dma((2, n_tp)),
        ],
        compiler_params=pltpu.CompilerParams(
            collective_id=1, has_side_effects=True, vmem_limit_bytes=56 * 1024 * 1024
        ),
        name="attend",
    )(query, keys, win_out, value_up_weight, out_win, out_lat)


def solution(mesh):
    return jax.shard_map(
        functools.partial(per_device, mesh.shape["sp"], mesh.shape["tp"]),
        mesh=mesh,
        in_specs=(
            P("sp", "tp"),
            P(),
            P(None, "tp"),
            P(None, "tp"),
            P(None, "tp"),
            P("tp"),
            P(None, "tp"),
            P(),
            P(),
            P(),
            P(None, "tp"),
            P(None, "tp"),
            P("tp", None),
            P("tp", None),
        ),
        out_specs=P("sp", "tp"),
        check_vma=False,
    )
```

time: 176 us -> 73.2 us (0.42)
  Pallas kernels: 0 us -> 67.2 us
  waiting for transfers between devices: 52.2 us -> 0 us
  matrix products: 46 us -> 0 us
  blocking collectives: 22.9 us -> 0 us
  other arithmetic: 21.9 us -> 1.95 us
  between operations: 13.4 us -> 0.03 us
  local copies, waits for them, and re-layouts: 14.9 us -> 3.82 us
  starting transfers between devices: 4.27 us -> 0 us
    pallas_call x0 -> x2, Pallas kernels: none -> 67.2 us  [the longest x1 40.7 us: per_device(): pl.pallas_call(functools.partial(project_kernel, n_sp, n_tp), out_shape=(...]
    dot_general x20 -> x0, matrix products: 46 us -> none  [the longest x6 12.6 us: per_device(): jnp.dot(normalized, weight, preferred_element_type=jnp.float32)]
    all_gather x2 -> x0, waiting for transfers between devices: 31.3 us -> none  [the longest x1 22.2 us: per_device(): lax.all_gather(activations, 'tp', axis=1, tiled=True).astype(jnp.float32)]
    all_gather x1 -> x0, blocking collectives: 22.9 us -> none  [per_device(): lax.all_gather(key_rotary, 'sp', axis=0, tiled=True)]
    reduce_scatter x1 -> x0, waiting for transfers between devices: 20.1 us -> none  [per_device(): lax.psum_scatter(terms.astype(jnp.bfloat16), 'tp', scatter_dimension=1, t...]
    reduce_sum x4 -> x0, other arithmetic: 12 us -> none  [the longest x2 9.28 us: latent_step(): totals = totals * factor + jnp.sum(weights, axis=2)]
    ppermute x2 -> x0, starting transfers between devices: 4.19 us -> none  [the longest x1 2.91 us: padded_2(): lax.ppermute(tail, axis, [(i, (i + 1) % count) for i in range(ends)])]
    while x19 -> x0, local copies, waits for them, and re-layouts: 3.67 us -> none  [the longest x1 2.04 us: over_blocks(): return lax.scan(one_block, running, stacked)[0]]
  transfers between devices with their start and end apart: 5 -> 0, of which waited for: 3 -> 0; matrix products, arithmetic and copies ran while one was open for 13% -> 0% of each run, Pallas kernels for 0% -> 0%
where the time goes in v1:
time: 73.2 us; the launch traced here: 73 us
  Pallas kernels  67.2 us (92%)
  local copies, waits for them, and re-layouts  3.82 us (5%)
  other arithmetic  1.95 us (3%)
    pallas_call x1, Pallas kernels, per_device(): pl.pallas_call(functools.partial(project_kernel, n_sp, n_tp), out_shape=(...  40.7 us
    pallas_call x1, Pallas kernels, per_device(): pl.pallas_call(functools.partial(attend_kernel, n_tp), out_shape=jax.Shap...  26.5 us
    unnamed x2, local copies, waits for them, and re-layouts  3.82 us

profile of v1, /device:TPU:0, one launch (start us, length us, event | category | flops | bytes accessed | tf_op | source)
XLA Modules:
  0.0 73.0 jit_solution(11872002709704182320)
XLA Ops:
  0.0 0.5 multiply_exponential_fusion.slope_ref
  0.6 0.5 fusion
  1.1 0.9 %pad_maximum_fusion = (f32[256,64]{1,0:T(8,128)}, f32[256,64]{1,0:T(8,128)}) fusion(f32[256,32]{1,0:T(8,128)S(1)} %get-tuple-element.13, f32[256,32]{1,0:T(8,128)S(1)} %get-tuple-element.12, f32[256,32]{1,0:T(8,128)S(1)} %get-tuple-element.11), kind=kLoop, calls=%fused_computation.2 | loop fusion | flops 32768 | bytes 229376 | tf_op jit(solution)/shard_map/concatenate | solution.py:326
  2.0 2.0 %copy.17.wr_hbm = bf16[2048,64]{1,0:T(8,128)(2,1)} copy(bf16[2048,64]{0,1:T(8,128)(2,1)} %param.22) | data formatting | bytes 524288 | tf_op args[8]
  3.9 40.7 %project.1 = (bf16[4,256,256]{2,1,0:T(8,128)(2,1)}, bf16[4096,256]{1,0:T(8,128)(2,1)}, bf16[256,512]{1,0:T(8,128)(2,1)}) custom-call(bf16[256,1024]{1,0:T(8,128)(2,1)} %x_ref.1, f32[4,1,512]{2,1,0:T(1,128)} %bitcast.2, f32[256,64]{1,0:T(8,128)} %get-tuple-element.14.cos_ref, f32[256,64]{1,0:T(8,128)} %get-tuple-element.15.sin_ref, f32[8]{0:T(128)} %sink_ref.1, ...), custom_call_target="tpu_custom_call" | custom-call | tf_op jit(solution)/shard_map/project/pallas_call | solution.py:338
  44.6 26.5 %attend.1 = bf16[256,1024]{1,0:T(8,128)(2,1)} custom-call(bf16[4,256,256]{2,1,0:T(8,128)(2,1)} %get-tuple-element.8.q_ref, bf16[4096,256]{1,0:T(8,128)(2,1)} %get-tuple-element.9.kv_ref, bf16[256,512]{1,0:T(8,128)(2,1)} %get-tuple-element.10.win_ref, bf16[128,512]{1,0:T(8,128)(2,1)} %vup_ref.1, bf16[512,2048]{1,0:T(8,128)(2,1)} %ow_hbm.1, ...), custom_call_target="tpu_custom_call" | custom-call | tf_op jit(solution)/shard_map/attend/pallas_call | solution.py:370
  71.1 1.9 %copy.19 = bf16[256,1024]{1,0:T(8,128)(2,1)} copy(bf16[256,1024]{1,0:T(8,128)(2,1)} %attend.1) | data formatting | bytes 1048576
  (2 shorter events, 0.0 us)

commit v2 on v1

--- a/solution.py
+++ b/solution.py
@@ -36,7 +36,7 @@
 
 def project_kernel(
     n_sp, n_tp,
-    x_ref, gain_ref, cos_ref, sin_ref, sink_ref, slope_ref, lng_ref, kup_ref,
+    x_ref, gain_ref, near_ref, base_ref, sink_ref, lng_ref, kup_ref,
     wkv_hbm, wr_hbm, wk_hbm, wv_hbm, wq_hbm, wlq_hbm,
     q_ref, kv_ref, win_ref,
     x_all, wkv, wr, wk, wv, wq, wlq, akv, ar, ak, av, aq, alq, sq, gath, halo, qwin,
@@ -87,7 +87,10 @@
     def add_in(block, slot, pairs, first):
         where = pl.ds(pl.multiple_of(slot * part, part), part)
         for weight, acc in pairs:
-            term = jnp.dot(block, weight[where, :], preferred_element_type=F32)
+            if weight is wr:
+                term = dot_nt(block, weight[:, where])
+            else:
+                term = jnp.dot(block, weight[where, :], preferred_element_type=F32)
             acc[...] = term if first else acc[...] + term
 
     def norm_block(raw, slot, first):
@@ -96,6 +99,12 @@
         sq[...] = total if first else sq[...] + total
         return (wide * gain_ref[slot]).astype(BF16)
 
+    near_cos, near_sin = near_ref[0], near_ref[1]
+    base_cos, base_sin = base_ref[sp, 0:1, :], base_ref[sp, 1:2, :]
+    cosine = near_cos * base_cos - near_sin * base_sin
+    plain_sine = near_sin * base_cos + near_cos * base_sin
+    lane = lax.broadcasted_iota(jnp.int32, plain_sine.shape, 1)
+    sine = jnp.where(lane < D_ROPE // 2, -plain_sine, plain_sine)
     small = ((wkv, akv), (wr, ar))
     big = ((wk, ak), (wv, av), (wq, aq), (wlq, alq))
     for load in loads:
@@ -118,7 +127,7 @@
     scale = lax.rsqrt(sq[:, 0:1] / (local * n_tp) + EPSILON)
     comp = akv[...]
     latent = comp * lax.rsqrt(jnp.mean(comp * comp, axis=1, keepdims=True) + EPSILON) * lng_ref[...]
-    rotary = turn(ar[...] * scale, cos_ref[...], sin_ref[...])
+    rotary = turn(ar[...] * scale, cosine, sine)
     gath[sp, 0:rows, :] = latent.astype(BF16)
     gath[sp, rows : rows + rows // 2, :] = jnp.concatenate(
         [rotary[: rows // 2], rotary[rows // 2 :]], axis=1
@@ -157,7 +166,7 @@
         one = alq[:, h * per_head : (h + 1) * per_head] * scale
         plain = one[:, :UNROTATED_WIDTH].astype(BF16)
         seen = dot_nt(plain, kup_ref[:, h * UNROTATED_WIDTH : (h + 1) * UNROTATED_WIDTH]) * factor
-        turned = turn(one[:, UNROTATED_WIDTH:], cos_ref[...], sin_ref[...]) * factor
+        turned = turn(one[:, UNROTATED_WIDTH:], cosine, sine) * factor
         q_ref[h, :, 0:UNROTATED_WIDTH] = seen.astype(BF16)
         q_ref[h, :, UNROTATED_WIDTH:] = jnp.concatenate([turned, jnp.zeros_like(turned)], axis=1).astype(BF16)
 
@@ -186,7 +195,9 @@
             for g in range(2):
                 head = kv_head * 2 + g
                 query = qwin[b * WINDOW : (b + 1) * WINDOW, head * DH : (head + 1) * DH]
-                scores = dot_nt(query, keys) * DH ** (-0.5) - slope_ref[head] * far
+                place = (tp * sink_ref.shape[0] + head + 1).astype(F32)
+                slope = jnp.exp2(jnp.full((1, span), -8.0 / HEADS_A, F32) * place)
+                scores = dot_nt(query, keys) * DH ** (-0.5) - slope * far
                 scores = jnp.where(inside, scores, -jnp.inf)
                 peak = jnp.maximum(jnp.max(scores, axis=1, keepdims=True), sink_ref[head])
                 weight = jnp.exp(scores - peak)
@@ -258,7 +269,7 @@
         peak[...] = jnp.full_like(peak, -jnp.inf)
 
         def step(i, carry):
-            keys = kv_ref[pl.ds(pl.multiple_of(i * chunk, chunk), chunk), :]
+            keys = kv_ref[pl.ds(i * chunk if isinstance(i, int) else pl.multiple_of(i * chunk, chunk), chunk), :]
             scores = dot_nt(query, keys)
             old = peak[:, 0:1]
             new = jnp.maximum(old, jnp.max(scores, axis=1, keepdims=True))
@@ -267,7 +278,12 @@
             peak[...] = jnp.broadcast_to(new, peak.shape)
             return carry
 
-        lax.fori_loop(0, kv_ref.shape[0] // chunk, step, 0)
+        count = kv_ref.shape[0] // chunk
+        if count > 4:
+            lax.fori_loop(0, count, step, 0)
+        else:
+            for i in range(count):
+                step(i, 0)
         bottom = acc[:, UNROTATED_WIDTH + D_ROPE : UNROTATED_WIDTH + D_ROPE + 1]
         blended = (acc[:, 0:VALUE_WIDTH] / bottom).astype(BF16)
         for h in range(heads):
@@ -319,19 +335,18 @@
     part = local // SUB
     heads_a = sink_logit.shape[0]
     heads_l = lat_query.shape[1] // (UNROTATED_WIDTH + D_ROPE)
-    places = (lax.axis_index("sp") * rows + jnp.arange(rows, dtype=jnp.int32)).astype(F32)
-    frequency = 1.0 / ROPE_BASE ** (jnp.arange(0, D_ROPE, 2).astype(F32) / D_ROPE)
-    angles = places[:, None] * frequency[None, :]
-    cosine, sine = jnp.cos(angles), jnp.sin(angles)
-    cosine = jnp.concatenate([cosine, cosine], axis=1)
-    sine = jnp.concatenate([-sine, sine], axis=1)
-    head_ids = lax.axis_index("tp") * heads_a + jnp.arange(heads_a, dtype=jnp.int32)
-    slopes = jnp.exp2(-8.0 * (head_ids + 1).astype(F32) / HEADS_A)
+    frequency = 1.0 / ROPE_BASE ** (np.arange(0, D_ROPE, 2) / D_ROPE)
+    frequency = np.concatenate([frequency, frequency])[None, :]
+    near = np.arange(rows)[:, None] * frequency
+    base = (np.arange(n_sp) * rows)[:, None] * frequency
+    near = jnp.asarray(np.stack([np.cos(near), np.sin(near)]), F32)
+    base = jnp.asarray(np.stack([np.cos(base), np.sin(base)], axis=1), F32)
 
     vmem = pl.BlockSpec(memory_space=pltpu.VMEM)
     smem = pl.BlockSpec(memory_space=pltpu.SMEM)
     hbm = pl.BlockSpec(memory_space=pl.ANY)
-    weights = (key_value_down_weight, rope_key, win_key, win_value, win_query, lat_query)
+    weights = (key_value_down_weight, rope_key.T, win_key, win_value, win_query, lat_query)
+    widths = [w.shape[0] if i == 1 else w.shape[1] for i, w in enumerate(weights)]
     hi = n_sp // 4
     dma = pltpu.SemaphoreType.DMA
     packed = rows + rows // 2
@@ -342,11 +357,11 @@
             jax.ShapeDtypeStruct((rows * n_sp, 2 * UNROTATED_WIDTH), BF16),
             jax.ShapeDtypeStruct((rows, heads_a * DH), BF16),
         ),
-        in_specs=[vmem, vmem, vmem, vmem, smem, smem, vmem, vmem] + [hbm] * 6,
+        in_specs=[vmem, vmem, vmem, vmem, smem, vmem, vmem] + [hbm] * 6,
         out_specs=(vmem, vmem, vmem),
         scratch_shapes=[pltpu.VMEM((n_tp * SUB, rows, part), BF16)]
         + [pltpu.VMEM(w.shape, BF16) for w in weights]
-        + [pltpu.VMEM((rows, w.shape[1]), F32) for w in weights]
+        + [pltpu.VMEM((rows, w), F32) for w in widths]
         + [
             pltpu.VMEM((rows, 128), F32),
             pltpu.VMEM((n_sp, packed, UNROTATED_WIDTH), BF16),
@@ -364,7 +379,7 @@
         ),
         name="project",
     )(
-        activations, norm_gain.reshape(n_tp * SUB, 1, part), cosine, sine, sink_logit, slopes,
+        activations, norm_gain.reshape(n_tp * SUB, 1, part), near, base, sink_logit,
         latent_norm_gain.reshape(1, -1), key_up_weight, *weights,
     )
     return pl.pallas_call(

time: 73.2 us -> 62.5 us (0.85)
  Pallas kernels: 67.2 us -> 60.4 us
  other arithmetic: 1.95 us -> 0 us
  local copies, waits for them, and re-layouts: 3.82 us -> 1.87 us
    pallas_call x1, Pallas kernels: 26.5 us -> 19.7 us  [per_device(): pl.pallas_call(functools.partial(attend_kernel, n_tp), out_shape=jax.Shap...]
    unnamed x2 -> x1, local copies, waits for them, and re-layouts: 3.82 us -> 1.87 us
    concatenate x1 -> x0, other arithmetic: 0.85 us -> none  [per_device(): cosine = jnp.concatenate([cosine, cosine], axis=1)]
where the time goes in v2:
time: 62.5 us; the launch traced here: 62.3 us
  Pallas kernels  60.4 us (97%)
  local copies, waits for them, and re-layouts  1.87 us (3%)
    pallas_call x1, Pallas kernels, per_device(): pl.pallas_call(functools.partial(project_kernel, n_sp, n_tp), out_shape=(...  40.6 us
    pallas_call x1, Pallas kernels, per_device(): pl.pallas_call(functools.partial(attend_kernel, n_tp), out_shape=jax.Shap...  19.7 us
    unnamed x1, local copies, waits for them, and re-layouts  1.87 us

profile of v2, /device:TPU:0, one launch (start us, length us, event | category | flops | bytes accessed | tf_op | source)
XLA Modules:
  0.0 62.3 jit_solution(3350640587487493553)
XLA Ops:
  0.0 40.6 %project.1 = (bf16[4,256,256]{2,1,0:T(8,128)(2,1)}, bf16[4096,256]{1,0:T(8,128)(2,1)}, bf16[256,512]{1,0:T(8,128)(2,1)}) custom-call(bf16[256,1024]{1,0:T(8,128)(2,1)} %x_ref.1, f32[4,1,512]{2,1,0:T(1,128)} %bitcast.4, f32[2,256,64]{2,1,0:T(8,128)} %constant.4.clone.near_ref, f32[16,2,64]{2,1,0:T(2,128)} %constant.5.clone.base_ref, f32[8]{0:T(128)} %sink_ref.1, ...), custom_call_target="tpu_custom_call" | custom-call | tf_op jit(solution)/shard_map/project/pallas_call | solution.py:353
  40.7 19.7 %attend.1 = bf16[256,1024]{1,0:T(8,128)(2,1)} custom-call(bf16[4,256,256]{2,1,0:T(8,128)(2,1)} %get-tuple-element.8.q_ref, bf16[4096,256]{1,0:T(8,128)(2,1)} %get-tuple-element.9.kv_ref, bf16[256,512]{1,0:T(8,128)(2,1)} %get-tuple-element.10.win_ref, bf16[128,512]{1,0:T(8,128)(2,1)} %vup_ref.1, bf16[512,2048]{1,0:T(8,128)(2,1)} %ow_hbm.1, ...), custom_call_target="tpu_custom_call" | custom-call | tf_op jit(solution)/shard_map/attend/pallas_call | solution.py:385
  60.4 1.9 %copy.18 = bf16[256,1024]{1,0:T(8,128)(2,1)} copy(bf16[256,1024]{1,0:T(8,128)(2,1)} %attend.1) | data formatting | bytes 1048576

commit v3 on v2

--- a/solution.py
+++ b/solution.py
@@ -22,6 +22,7 @@
 F32 = jnp.float32
 BF16 = jnp.bfloat16
 SUB = 2
+BANDS = 4
 
 
 def turn(vectors, cosine, sine):
@@ -251,7 +252,7 @@
     sp = lax.axis_index("sp")
     tp = lax.axis_index("tp")
     heads, rows, _ = q_ref.shape
-    half = rows // 2
+    half = rows // BANDS
     cols = out_ref.shape[1]
     loads = [pltpu.make_async_copy(ow_hbm, ow, w_sem.at[0]), pltpu.make_async_copy(ol_hbm, ol, w_sem.at[1])]
     for load in loads:
@@ -263,7 +264,7 @@
 
     chunk = min(1024, kv_ref.shape[0])
     copies = []
-    for b in range(2):
+    for b in range(BANDS):
         query = jnp.concatenate([q_ref[h, b * half : (b + 1) * half, :] for h in range(heads)], axis=0)
         acc[...] = jnp.zeros_like(acc)
         peak[...] = jnp.full_like(peak, -jnp.inf)
@@ -316,7 +317,7 @@
             copy.start()
             copies.append((b, s, copy))
         own[b] = terms(tp)
-    for b in range(2):
+    for b in range(BANDS):
         total = own[b]
         for bb, s, copy in copies:
             if bb == b:
@@ -390,14 +391,14 @@
         scratch_shapes=[
             pltpu.VMEM(out_win.shape, BF16),
             pltpu.VMEM(out_lat.shape, BF16),
-            pltpu.VMEM((heads_l * rows // 2, 2 * UNROTATED_WIDTH), F32),
-            pltpu.VMEM((heads_l * rows // 2, 128), F32),
-            pltpu.VMEM((rows // 2, heads_l * VALUE_WIDTH), BF16),
-            pltpu.VMEM((2, n_tp - 1, rows // 2, width // n_tp), BF16),
-            pltpu.VMEM((2, n_tp - 1, rows // 2, width // n_tp), BF16),
-            pltpu.VMEM((2, rows // 2, width // n_tp), F32),
+            pltpu.VMEM((heads_l * rows // BANDS, 2 * UNROTATED_WIDTH), F32),
+            pltpu.VMEM((heads_l * rows // BANDS, 128), F32),
+            pltpu.VMEM((rows // BANDS, heads_l * VALUE_WIDTH), BF16),
+            pltpu.VMEM((BANDS, n_tp - 1, rows // BANDS, width // n_tp), BF16),
+            pltpu.VMEM((BANDS, n_tp - 1, rows // BANDS, width // n_tp), BF16),
+            pltpu.VMEM((BANDS, rows // BANDS, width // n_tp), F32),
             dma((2,)),
-            dma((2, n_tp)), dma((2, n_tp)),
+            dma((BANDS, n_tp)), dma((BANDS, n_tp)),
         ],
         compiler_params=pltpu.CompilerParams(
             collective_id=1, has_side_effects=True, vmem_limit_bytes=56 * 1024 * 1024

time: 62.5 us -> 62.1 us (level)
  no operation moved by 1% of the time
where the time goes in v3:
time: 62.1 us; the launch traced here: 61.9 us
  Pallas kernels  60 us (97%)
  local copies, waits for them, and re-layouts  1.87 us (3%)
    pallas_call x1, Pallas kernels, per_device(): pl.pallas_call(functools.partial(project_kernel, n_sp, n_tp), out_shape=(...  40.6 us
    pallas_call x1, Pallas kernels, per_device(): pl.pallas_call(functools.partial(attend_kernel, n_tp), out_shape=jax.Shap...  19.3 us
    unnamed x1, local copies, waits for them, and re-layouts  1.87 us

profile of v3, /device:TPU:0, one launch (start us, length us, event | category | flops | bytes accessed | tf_op | source)
XLA Modules:
  0.0 61.9 jit_solution(2751759103318415834)
XLA Ops:
  0.0 40.6 %project.1 = (bf16[4,256,256]{2,1,0:T(8,128)(2,1)}, bf16[4096,256]{1,0:T(8,128)(2,1)}, bf16[256,512]{1,0:T(8,128)(2,1)}) custom-call(bf16[256,1024]{1,0:T(8,128)(2,1)} %x_ref.1, f32[4,1,512]{2,1,0:T(1,128)} %bitcast.4, f32[2,256,64]{2,1,0:T(8,128)} %constant.4.clone.near_ref, f32[16,2,64]{2,1,0:T(2,128)} %constant.5.clone.base_ref, f32[8]{0:T(128)} %sink_ref.1, ...), custom_call_target="tpu_custom_call" | custom-call | tf_op jit(solution)/shard_map/project/pallas_call | solution.py:354
  40.7 19.3 %attend.1 = bf16[256,1024]{1,0:T(8,128)(2,1)} custom-call(bf16[4,256,256]{2,1,0:T(8,128)(2,1)} %get-tuple-element.8.q_ref, bf16[4096,256]{1,0:T(8,128)(2,1)} %get-tuple-element.9.kv_ref, bf16[256,512]{1,0:T(8,128)(2,1)} %get-tuple-element.10.win_ref, bf16[128,512]{1,0:T(8,128)(2,1)} %vup_ref.1, bf16[512,2048]{1,0:T(8,128)(2,1)} %ow_hbm.1, ...), custom_call_target="tpu_custom_call" | custom-call | tf_op jit(solution)/shard_map/attend/pallas_call | solution.py:386
  60.0 1.9 %copy.18 = bf16[256,1024]{1,0:T(8,128)(2,1)} copy(bf16[256,1024]{1,0:T(8,128)(2,1)} %attend.1) | data formatting | bytes 1048576
